TPU v7x, 256 devices: a whole 4x4x8 slice. The times are simulated.
256 devices in a mesh: fs: 64 (over z, y, core), tp: 4 (over x).
Axes of the slice: x: 4, y: 4, z: 8, core: 2. Of those that a mesh axis runs over, the one named last changes fastest.
Arguments:
- tokens: bfloat16 [65536, 2048], P('fs', 'tp'), may hold values from -6 to 6
- norm_gain: float32 [2048], P('fs'), may hold values from 0.1 to 1.9
- up_master: float32 [2048, 4096], P('fs', 'tp'), may hold values from -0.125 to 0.125
- down_master: float32 [4096, 2048], P('fs', 'tp'), may hold values from -0.09375 to 0.09375
Outputs:
- mixed: bfloat16 [65536, 2048], P('fs', 'tp')
- up_ready: bfloat16 [2048, 4096], P(None, 'tp')
- down_ready: bfloat16 [4096, 2048], P('tp')
All inputs are finite; a program needn't handle non-finite values.
Results may differ from a plain program's by a relative error of at most 0.0095.
Values may be sent and summed in bfloat16 or wider, within the bound.
A program may use at most 128 MiB of HBM per device.

v0:
```python
import jax
import jax.numpy as jnp
from jax import lax
from jax.sharding import Mesh
from jax.sharding import PartitionSpec as P

FS = ("fs_0", "fs_1", "fs_2")


def sent_to_all(shard, axis):
    peers = lax.axis_size(axis)
    return lax.all_to_all(
        jnp.broadcast_to(shard[None], (peers, *shard.shape)), axis, 0, 0, tiled=True
    )


def laid_out(pieces, dim):
    lengths = list(pieces.shape[1:])
    lengths[dim] *= pieces.shape[0]
    return jnp.moveaxis(pieces, 0, dim).reshape(lengths)


def gathered_by_axis(shard, axes, dim):
    far, near = axes
    initial = sent_to_all(shard, far)
    pieces = jnp.swapaxes(sent_to_all(initial, near), 0, 1)
    return laid_out(pieces.reshape(-1, *shard.shape), dim)


def gather_directly(shard, axis, dim):
    return laid_out(sent_to_all(shard, axis), dim)


def shards(tokens, norm_gain, up_master, down_master):
    group_size = lax.axis_size("tp")
    group_index = lax.axis_index("tp")
    up_local = (norm_gain[:, None] * up_master).astype(jnp.bfloat16)
    up_ready = gathered_by_axis(up_local, (("fs_0", "fs_1"), "fs_2"), 0)
    down_local = down_master.astype(jnp.bfloat16)
    wide_rows = lax.all_gather(down_local, "tp", axis=1, tiled=True)
    whole_down = lax.all_gather(wide_rows, FS, axis=0, tiled=True)
    row_count = whole_down.shape[0] // group_size
    down_ready = lax.dynamic_slice_in_dim(whole_down, group_index * row_count, row_count, 0)
    features = gather_directly(tokens, "tp", 1)
    values = features.astype(jnp.float32)
    mean_square = jnp.mean(values * values, axis=-1, keepdims=True)
    normed = (values * lax.rsqrt(mean_square + 1e-06)).astype(jnp.bfloat16)
    before = jnp.dot(normed, up_ready, preferred_element_type=jnp.float32)
    hidden = jnp.square(jax.nn.relu(before)).astype(jnp.bfloat16)
    partial_value = jnp.dot(hidden, down_ready, preferred_element_type=jnp.float32)
    mixed = lax.psum_scatter(
        partial_value.astype(jnp.bfloat16), "tp", scatter_dimension=1, tiled=True
    )
    return (mixed, up_ready, down_ready)


def solution(mesh):
    finer = Mesh(mesh.devices.reshape(8, 4, 2, mesh.shape["tp"]), ("fs_0", "fs_1", "fs_2", "tp"))
    placed = (P(FS, "tp"), P(FS), P(FS, "tp"), P(FS, "tp"))
    return jax.shard_map(
        shards,
        mesh=finer,
        in_specs=placed,
        out_specs=(P(FS, "tp"), P(None, "tp"), P("tp", None)),
        check_vma=False,
    )
```

profile of v0, /device:TPU:1, one launch (start us, length us, event | category | flops | bytes accessed | tf_op | source)
XLA Modules:
  0.0 243.9 jit_solution(11935646034167226579)
XLA Ops:
  7.2 0.0 all-gather.2.cloned.1.call-start
  7.2 0.9 convert_element_type.33
  8.1 11.8 %all_gather.6 = bf16[64,2048]{1,0:T(8,128)(2,1)} all-gather(bf16[64,512]{1,0:T(8,128)(2,1)S(1)} %convert_element_type.33), channel_id=1, replica_groups=mesh['fs_0'=8,'fs_1'=4,'fs_2'=2,'tp'=4] {'tp'}, dimensions={1}, use_global_device_ids=true | all-gather | bytes 327680 | tf_op jit(solution)/shard_map/all_gather | solution.py:40
  19.9 0.0 all-gather.2.cloned.1.call-update
  20.0 1.5 copy.9
  21.5 2.6 %broadcast_in_dim.6 = bf16[4,1024,512]{1,2,0:T(8,128)(2,1)} broadcast(bf16[1024,512]{0,1:T(8,128)(2,1)S(1)} %copy.9), dimensions={1,2} | broadcast | bytes 5242880 | tf_op jit(solution)/shard_map/broadcast_in_dim | solution.py:13
  24.0 0.0 copy-start
  24.0 0.0 copy-start.1
  24.0 5.0 %all-to-all-start = ((bf16[4,1024,512]{1,2,0:T(8,128)(2,1)}), bf16[4,1024,512]{1,2,0:T(8,128)(2,1)}, u32[]{:S(2)}, u32[]{:S(2)}) async-start(bf16[4,1024,512]{1,2,0:T(8,128)(2,1)} %broadcast_in_dim.6), calls=%async_computation | async-start | bytes 8388608 | tf_op jit(solution)/shard_map/all_to_all | solution.py:12
  29.0 0.0 copy-done
  29.0 0.0 copy-done.1
  29.0 0.1 multiply_convert_fusion.1
  29.1 44.2 %all-to-all-done = bf16[4,1024,512]{1,2,0:T(8,128)(2,1)} async-done(((bf16[4,1024,512]{1,2,0:T(8,128)(2,1)}), bf16[4,1024,512]{1,2,0:T(8,128)(2,1)}, u32[]{:S(2)}, u32[]{:S(2)}) %all-to-all-start) | async-done | bytes 4194336 | tf_op jit(solution)/shard_map/all_to_all | solution.py:12
  73.4 1.6 broadcast_in_dim.7
  74.9 12.8 %all-to-all-start.1 = ((bf16[32,32,1024]{2,1,0:T(8,128)(2,1)}), bf16[32,32,1024]{2,1,0:T(8,128)(2,1)S(1)}, u32[]{:S(2)}, u32[]{:S(2)}) async-start(bf16[32,32,1024]{2,1,0:T(8,128)(2,1)} %broadcast_in_dim.7), calls=%async_computation.1 | async-start | bytes 4194304 | tf_op jit(solution)/shard_map/all_to_all | solution.py:12
  87.7 0.0 reduce-scatter.2.cloned.1.call-start
  87.8 3.2 %fusion = f32[1024]{0:T(1024)S(1)} fusion(bf16[4,1024,512]{1,2,0:T(8,128)(2,1)} %all-to-all-done), kind=kLoop, calls=%fused_computation.2 | loop fusion | flops 6290432 | bytes 4198400 | tf_op jit(solution)/shard_map/reduce_sum | solution.py:46
  91.0 5.5 %fusion.1 = bf16[4,1024,512]{1,2,0:T(8,128)(2,1)} fusion(bf16[4,1024,512]{1,2,0:T(8,128)(2,1)} %all-to-all-done, f32[1024]{0:T(1024)S(1)} %add_rsqrt_fusion), kind=kLoop, calls=%fused_computation.3 | loop fusion | flops 6291456 | bytes 8392704 | tf_op jit(solution)/shard_map/convert_element_type | solution.py:47
  96.5 61.2 %all-to-all-done.1 = bf16[32,32,1024]{2,1,0:T(8,128)(2,1)S(1)} async-done(((bf16[32,32,1024]{2,1,0:T(8,128)(2,1)}), bf16[32,32,1024]{2,1,0:T(8,128)(2,1)S(1)}, u32[]{:S(2)}, u32[]{:S(2)}) %all-to-all-start.1) | async-done | bytes 2097184 | tf_op jit(solution)/shard_map/all_to_all | solution.py:12
  157.6 0.5 broadcast_in_dim.8
  158.2 13.2 %all_to_all.15 = bf16[2,32,32,1024]{3,2,1,0:T(8,128)(2,1)S(1)} all-to-all(bf16[2,32,32,1024]{3,2,1,0:T(8,128)(2,1)S(1)} %broadcast_in_dim.8), channel_id=1, replica_groups=mesh['fs_0'=8,'fs_1'=4,'fs_2'=2,'tp'=4] {'fs_2'}, dimensions={0} | all-to-all | bytes 8388608 | tf_op jit(solution)/shard_map/all_to_all | solution.py:12
  171.4 2.5 %copy.10 = bf16[2,32,32,1024]{3,2,0,1:T(8,128)(2,1)} copy(bf16[2,32,32,1024]{3,2,1,0:T(8,128)(2,1)S(1)} %all_to_all.15) | data formatting | bytes 8388608 | tf_op jit(solution)/shard_map/all_to_all | solution.py:12
  173.9 0.0 all-gather.2.cloned.1.call-done
  173.9 4.8 %constant_dynamic-slice_fusion = bf16[1024,2048]{1,0:T(8,128)(2,1)} fusion(bf16[4096,2048]{1,0:T(8,128)(2,1)} %all-gather.2.cloned.1.call-done, s32[]{:T(128)S(6)} %select_n.3), kind=kLoop, calls=%fused_computation.8 | loop fusion | bytes 8388612 | tf_op jit(solution)/shard_map/dynamic_slice | solution.py:43
  178.6 14.4 %convolution_convert_fusion = bf16[1024,2048]{1,0:T(8,128)(2,1)} fusion(bf16[1024,2048]{1,0:T(8,128)(2,1)} %constant_dynamic-slice_fusion, bf16[1024,2048]{0,1:T(8,128)(2,1)} %bitcast.11, bf16[2048,1024]{1,0:T(8,128)(2,1)} %bitcast.9), kind=kOutput, calls=%fused_computation.5 | convolution fusion | flops 8595177472 | bytes 16777216 | tf_op jit(solution)/shard_map/dot_general | solution.py:50
  193.0 0.0 reduce-scatter.2.cloned.1.call-update
  193.1 44.0 %reduce-scatter.2.cloned.1.call-done = bf16[1024,512]{1,0:T(8,128)(2,1)} async-done(((bf16[1024,2048]{1,0:T(8,128)(2,1)}), bf16[1024,512]{1,0:T(8,128)(2,1)}) %reduce-scatter.2.cloned.1.call-update) | async-done | bytes 1048592 | tf_op jit(solution)/shard_map/reduce_scatter | solution.py:51
  (1 shorter events, 0.0 us)
Async XLA Ops:
  7.2 166.7 %all-gather.2.cloned.1.call-start = ((), (), s32[]{:S(2)}) async-start(), calls=%async_computation.4 | async-start | bytes 17039360 | tf_op jit(solution)/shard_map/all_gather | solution.py:41
  24.0 5.0 %copy-start = (f32[32,1024]{1,0:T(8,128)S(1)}, f32[32,1024]{1,0:T(8,128)}, u32[]{:S(2)}) copy-start(f32[32,1024]{1,0:T(8,128)} %param.6) | copy-start | bytes 393220
  24.0 5.0 %copy-start.1 = (f32[32]{0:T(128)S(1)}, f32[32]{0:T(128)}, u32[]{:S(2)}) copy-start(f32[32]{0:T(128)} %param.5) | copy-start | bytes 388
  24.0 49.3 %all-to-all-start = ((bf16[4,1024,512]{1,2,0:T(8,128)(2,1)}), bf16[4,1024,512]{1,2,0:T(8,128)(2,1)}, u32[]{:S(2)}, u32[]{:S(2)}) async-start(bf16[4,1024,512]{1,2,0:T(8,128)(2,1)} %broadcast_in_dim.6), calls=%async_computation | async-start | bytes 8388608 | tf_op jit(solution)/shard_map/all_to_all | solution.py:12
  74.9 82.7 %all-to-all-start.1 = ((bf16[32,32,1024]{2,1,0:T(8,128)(2,1)}), bf16[32,32,1024]{2,1,0:T(8,128)(2,1)S(1)}, u32[]{:S(2)}, u32[]{:S(2)}) async-start(bf16[32,32,1024]{2,1,0:T(8,128)(2,1)} %broadcast_in_dim.7), calls=%async_computation.1 | async-start | bytes 4194304 | tf_op jit(solution)/shard_map/all_to_all | solution.py:12
  87.7 149.3 %reduce-scatter.2.cloned.1.call-start = ((), (), s32[]{:S(2)}) async-start(), calls=%async_computation.5 | async-start | bytes 5242880 | tf_op jit(solution)/shard_map/reduce_scatter | solution.py:51
Sparse Core Ops, SparseCore 0:
  20.1 148.1 all-gather.1
  193.2 43.8 reduce-scatter.1
where the time goes:
time: 244 us
  waiting for transfers between devices  149 us (61%)
  blocking collectives  25.1 us (10%)
  starting transfers between devices  17.9 us (7%)
  matrix products  14.4 us (6%)
  between operations  14.1 us (6%)
  local copies, waits for them, and re-layouts  13.4 us (5%)
  other arithmetic  9.67 us (4%)
    all_to_all x2, waiting for transfers between devices, sent_to_all(): lax.all_to_all(jnp.broadcast_to(shard[None], (peers, *shard.shape)), axis...  105 us
    reduce_scatter x1, waiting for transfers between devices, shards(): lax.psum_scatter(partial_value.astype(jnp.bfloat16), 'tp', scatter_dimens...  44 us
    all_to_all x2, starting transfers between devices, sent_to_all(): lax.all_to_all(jnp.broadcast_to(shard[None], (peers, *shard.shape)), axis...  17.8 us
    dot_general x1, matrix products, shards(): jnp.dot(hidden, down_ready, preferred_element_type=jnp.float32)  14.4 us
    all_to_all x1, blocking collectives, sent_to_all(): lax.all_to_all(jnp.broadcast_to(shard[None], (peers, *shard.shape)), axis...  13.2 us
    all_gather x1, blocking collectives, shards(): wide_rows = lax.all_gather(down_local, 'tp', axis=1, tiled=True)  11.8 us
    convert_element_type x1, other arithmetic, shards(): normed = (values * lax.rsqrt(mean_square + 1e-06)).astype(jnp.bfloat16)  5.48 us
  transfers between devices with their start and end apart: 4, of which 3 were waited for; matrix products, arithmetic and copies ran while one was open for 7% of the time, Pallas kernels for 0%

commit v1 on v0

--- a/solution.py
+++ b/solution.py
@@ -5,6 +5,13 @@
 from jax.sharding import PartitionSpec as P
 
 FS = ("fs_0", "fs_1", "fs_2")
+
+
+def exchange_gather(block, name, d):
+    count = lax.axis_size(name)
+    blocks = jnp.stack([block for _ in range(count)])
+    blocks = lax.all_to_all(blocks, name, split_axis=0, concat_axis=0)
+    return jnp.concatenate(blocks, axis=d)
 
 
 def sent_to_all(shard, axis):
@@ -37,7 +44,7 @@
     up_local = (norm_gain[:, None] * up_master).astype(jnp.bfloat16)
     up_ready = gathered_by_axis(up_local, (("fs_0", "fs_1"), "fs_2"), 0)
     down_local = down_master.astype(jnp.bfloat16)
-    wide_rows = lax.all_gather(down_local, "tp", axis=1, tiled=True)
+    wide_rows = exchange_gather(down_local, "tp", 1)
     whole_down = lax.all_gather(wide_rows, FS, axis=0, tiled=True)
     row_count = whole_down.shape[0] // group_size
     down_ready = lax.dynamic_slice_in_dim(whole_down, group_index * row_count, row_count, 0)

time: 244 us -> 244 us (level)
  waiting for transfers between devices: 149 us -> 153 us
  blocking collectives: 25.1 us -> 21.5 us
    all_gather x1 -> x0, blocking collectives: 11.8 us -> none  [shards(): wide_rows = lax.all_gather(down_local, 'tp', axis=1, tiled=True)]
    all_to_all x0 -> x1, blocking collectives: none -> 10.2 us  [exchange_gather(): blocks = lax.all_to_all(blocks, name, split_axis=0, concat_axis=0)]
    all_to_all x2, waiting for transfers between devices: 105 us -> 110 us  [sent_to_all(): lax.all_to_all(jnp.broadcast_to(shard[None], (peers, *shard.shape)), axis...]
where the time goes in v1:
time: 244 us; the launch traced here: 243 us
  waiting for transfers between devices  153 us (63%)
  blocking collectives  21.5 us (9%)
  starting transfers between devices  16.3 us (7%)
  matrix products  14.4 us (6%)
  local copies, waits for them, and re-layouts  14.1 us (6%)
  between operations  14.1 us (6%)
  other arithmetic  9.58 us (4%)
    all_to_all x2, waiting for transfers between devices, sent_to_all(): lax.all_to_all(jnp.broadcast_to(shard[None], (peers, *shard.shape)), axis...  110 us
    reduce_scatter x1, waiting for transfers between devices, shards(): lax.psum_scatter(partial_value.astype(jnp.bfloat16), 'tp', scatter_dimens...  43.6 us
    all_to_all x2, starting transfers between devices, sent_to_all(): lax.all_to_all(jnp.broadcast_to(shard[None], (peers, *shard.shape)), axis...  16.2 us
    dot_general x1, matrix products, shards(): jnp.dot(hidden, down_ready, preferred_element_type=jnp.float32)  14.4 us
    all_to_all x1, blocking collectives, sent_to_all(): lax.all_to_all(jnp.broadcast_to(shard[None], (peers, *shard.shape)), axis...  11.3 us
    all_to_all x1, blocking collectives, exchange_gather(): blocks = lax.all_to_all(blocks, name, split_axis=0, concat_axis=0)  10.2 us
    convert_element_type x1, other arithmetic, shards(): normed = (values * lax.rsqrt(mean_square + 1e-06)).astype(jnp.bfloat16)  5.44 us
  transfers between devices with their start and end apart: 4, of which 3 were waited for; matrix products, arithmetic and copies ran while one was open for 7% of the time, Pallas kernels for 0%

profile of v1, /device:TPU:1, one launch (start us, length us, event | category | flops | bytes accessed | tf_op | source)
XLA Modules:
  0.0 243.3 jit_solution(8823815695074514513)
XLA Ops:
  7.2 0.0 all-gather.2.cloned.1.call-start
  7.2 0.9 convert_element_type.33
  8.2 10.2 %all_to_all.20 = bf16[4,64,512]{2,1,0:T(8,128)(2,1)S(1)} all-to-all(bf16[4,64,512]{2,1,0:T(8,128)(2,1)S(1)} %stack.2), channel_id=1, replica_groups=mesh['fs_0'=8,'fs_1'=4,'fs_2'=2,'tp'=4] {'tp'}, dimensions={0} | all-to-all | bytes 524288 | tf_op jit(solution)/shard_map/all_to_all | solution.py:13
  18.3 0.7 copy.12
  19.1 0.0 all-gather.2.cloned.1.call-update
  19.1 1.5 copy.9
  20.6 2.6 %broadcast_in_dim.6 = bf16[4,1024,512]{1,2,0:T(8,128)(2,1)} broadcast(bf16[1024,512]{0,1:T(8,128)(2,1)S(1)} %copy.9), dimensions={1,2} | broadcast | bytes 5242880 | tf_op jit(solution)/shard_map/broadcast_in_dim | solution.py:20
  23.1 0.0 copy-start
  23.2 0.0 copy-start.1
  23.2 5.0 %all-to-all-start = ((bf16[4,1024,512]{1,2,0:T(8,128)(2,1)}), bf16[4,1024,512]{1,2,0:T(8,128)(2,1)}, u32[]{:S(2)}, u32[]{:S(2)}) async-start(bf16[4,1024,512]{1,2,0:T(8,128)(2,1)} %broadcast_in_dim.6), calls=%async_computation | async-start | bytes 8388608 | tf_op jit(solution)/shard_map/all_to_all | solution.py:19
  28.1 0.0 copy-done
  28.1 0.0 copy-done.1
  28.2 0.1 multiply_convert_fusion.1
  28.2 46.8 %all-to-all-done = bf16[4,1024,512]{1,2,0:T(8,128)(2,1)} async-done(((bf16[4,1024,512]{1,2,0:T(8,128)(2,1)}), bf16[4,1024,512]{1,2,0:T(8,128)(2,1)}, u32[]{:S(2)}, u32[]{:S(2)}) %all-to-all-start) | async-done | bytes 4194336 | tf_op jit(solution)/shard_map/all_to_all | solution.py:19
  75.0 1.6 broadcast_in_dim.7
  76.6 11.2 %all-to-all-start.1 = ((bf16[32,32,1024]{2,1,0:T(8,128)(2,1)}), bf16[32,32,1024]{2,1,0:T(8,128)(2,1)S(1)}, u32[]{:S(2)}, u32[]{:S(2)}) async-start(bf16[32,32,1024]{2,1,0:T(8,128)(2,1)} %broadcast_in_dim.7), calls=%async_computation.1 | async-start | bytes 4194304 | tf_op jit(solution)/shard_map/all_to_all | solution.py:19
  87.8 0.0 reduce-scatter.2.cloned.1.call-start
  87.9 3.1 %fusion = f32[1024]{0:T(1024)S(1)} fusion(bf16[4,1024,512]{1,2,0:T(8,128)(2,1)} %all-to-all-done), kind=kLoop, calls=%fused_computation.2 | loop fusion | flops 6290432 | bytes 4198400 | tf_op jit(solution)/shard_map/reduce_sum | solution.py:53
  91.0 5.4 %fusion.1 = bf16[4,1024,512]{1,2,0:T(8,128)(2,1)} fusion(bf16[4,1024,512]{1,2,0:T(8,128)(2,1)} %all-to-all-done, f32[1024]{0:T(1024)S(1)} %add_rsqrt_fusion), kind=kLoop, calls=%fused_computation.3 | loop fusion | flops 6291456 | bytes 8392704 | tf_op jit(solution)/shard_map/convert_element_type | solution.py:54
  96.4 62.9 %all-to-all-done.1 = bf16[32,32,1024]{2,1,0:T(8,128)(2,1)S(1)} async-done(((bf16[32,32,1024]{2,1,0:T(8,128)(2,1)}), bf16[32,32,1024]{2,1,0:T(8,128)(2,1)S(1)}, u32[]{:S(2)}, u32[]{:S(2)}) %all-to-all-start.1) | async-done | bytes 2097184 | tf_op jit(solution)/shard_map/all_to_all | solution.py:19
  159.4 0.5 broadcast_in_dim.8
  159.9 11.3 %all_to_all.21 = bf16[2,32,32,1024]{3,2,1,0:T(8,128)(2,1)S(1)} all-to-all(bf16[2,32,32,1024]{3,2,1,0:T(8,128)(2,1)S(1)} %broadcast_in_dim.8), channel_id=1, replica_groups=mesh['fs_0'=8,'fs_1'=4,'fs_2'=2,'tp'=4] {'fs_2'}, dimensions={0} | all-to-all | bytes 8388608 | tf_op jit(solution)/shard_map/all_to_all | solution.py:19
  171.2 2.5 %copy.10 = bf16[2,32,32,1024]{3,2,0,1:T(8,128)(2,1)} copy(bf16[2,32,32,1024]{3,2,1,0:T(8,128)(2,1)S(1)} %all_to_all.21) | data formatting | bytes 8388608 | tf_op jit(solution)/shard_map/all_to_all | solution.py:19
  173.7 0.0 all-gather.2.cloned.1.call-done
  173.7 4.8 %constant_dynamic-slice_fusion = bf16[1024,2048]{1,0:T(8,128)(2,1)} fusion(bf16[4096,2048]{1,0:T(8,128)(2,1)} %all-gather.2.cloned.1.call-done, s32[]{:T(128)S(6)} %select_n.3), kind=kLoop, calls=%fused_computation.8 | loop fusion | bytes 8388612 | tf_op jit(solution)/shard_map/dynamic_slice | solution.py:50
  178.5 14.4 %convolution_convert_fusion = bf16[1024,2048]{1,0:T(8,128)(2,1)} fusion(bf16[1024,2048]{1,0:T(8,128)(2,1)} %constant_dynamic-slice_fusion, bf16[1024,2048]{0,1:T(8,128)(2,1)} %bitcast.14, bf16[2048,1024]{1,0:T(8,128)(2,1)} %bitcast.12), kind=kOutput, calls=%fused_computation.5 | convolution fusion | flops 8595177472 | bytes 16777216 | tf_op jit(solution)/shard_map/dot_general | solution.py:57
  192.9 0.0 reduce-scatter.2.cloned.1.call-update
  192.9 43.6 %reduce-scatter.2.cloned.1.call-done = bf16[1024,512]{1,0:T(8,128)(2,1)} async-done(((bf16[1024,2048]{1,0:T(8,128)(2,1)}), bf16[1024,512]{1,0:T(8,128)(2,1)}) %reduce-scatter.2.cloned.1.call-update) | async-done | bytes 1048592 | tf_op jit(solution)/shard_map/reduce_scatter | solution.py:58
  (2 shorter events, 0.0 us)
Async XLA Ops:
  7.2 166.5 %all-gather.2.cloned.1.call-start = ((), (), s32[]{:S(2)}) async-start(), calls=%async_computation.5 | async-start | bytes 17039360 | tf_op jit(solution)/shard_map/all_gather | solution.py:48
  23.1 5.0 %copy-start = (f32[32,1024]{1,0:T(8,128)S(1)}, f32[32,1024]{1,0:T(8,128)}, u32[]{:S(2)}) copy-start(f32[32,1024]{1,0:T(8,128)} %param.6) | copy-start | bytes 393220
  23.2 5.0 %copy-start.1 = (f32[32]{0:T(128)S(1)}, f32[32]{0:T(128)}, u32[]{:S(2)}) copy-start(f32[32]{0:T(128)} %param.5) | copy-start | bytes 388
  23.2 51.9 %all-to-all-start = ((bf16[4,1024,512]{1,2,0:T(8,128)(2,1)}), bf16[4,1024,512]{1,2,0:T(8,128)(2,1)}, u32[]{:S(2)}, u32[]{:S(2)}) async-start(bf16[4,1024,512]{1,2,0:T(8,128)(2,1)} %broadcast_in_dim.6), calls=%async_computation | async-start | bytes 8388608 | tf_op jit(solution)/shard_map/all_to_all | solution.py:19
  76.6 82.8 %all-to-all-start.1 = ((bf16[32,32,1024]{2,1,0:T(8,128)(2,1)}), bf16[32,32,1024]{2,1,0:T(8,128)(2,1)S(1)}, u32[]{:S(2)}, u32[]{:S(2)}) async-start(bf16[32,32,1024]{2,1,0:T(8,128)(2,1)} %broadcast_in_dim.7), calls=%async_computation.1 | async-start | bytes 4194304 | tf_op jit(solution)/shard_map/all_to_all | solution.py:19
  87.8 148.7 %reduce-scatter.2.cloned.1.call-start = ((), (), s32[]{:S(2)}) async-start(), calls=%async_computation.6 | async-start | bytes 5242880 | tf_op jit(solution)/shard_map/reduce_scatter | solution.py:58
Sparse Core Ops, SparseCore 0:
  19.2 147.1 all-gather.1
  193.0 43.3 reduce-scatter.1
